TPU v7x, 32 devices: a whole 2x2x4 slice. The times are simulated.
32 devices in a mesh: grp: 2 (over y), sp: 4 (over z), tp: 4 (over x, core).
Axes of the slice: x: 2, y: 2, z: 4, core: 2. Of those that a mesh axis runs over, the one named last changes fastest.
Arguments:
- window_query: bfloat16 [2560, 2048], P(('grp', 'sp'), 'tp'), parts along dimension 0, may hold values from -24 to 24
- window_key: bfloat16 [2560, 1024], P(('grp', 'sp'), 'tp'), parts along dimension 0, may hold values from -24 to 24
- window_value: bfloat16 [2560, 1024], P(('grp', 'sp'), 'tp'), parts along dimension 0, may hold values from -6 to 6
- grid_query: bfloat16 [2560, 2048], P(('grp', 'sp'), 'tp'), parts along dimension 0, may hold values from -10 to 10
- grid_key: bfloat16 [2560, 1024], P(('grp', 'sp'), 'tp'), parts along dimension 0, may hold values from -10 to 10
- grid_value: bfloat16 [2560, 1024], P(('grp', 'sp'), 'tp'), parts along dimension 0, may hold values from -6 to 6
- sink_logit: float32 [16], P('tp'), may hold values from 1 to 6
- query_gain: float32 [128], replicated, may hold values from 0.8 to 6
- key_gain: float32 [128], replicated, may hold values from 0.8 to 6
- window_weights: bfloat16 [2048, 4096], P('tp'), may hold values from -0.59765625 to 0.59765625
- grid_weights: bfloat16 [2048, 4096], P('tp'), may hold values from -0.59765625 to 0.59765625
Outputs:
- merged: bfloat16 [2560, 4096], P(('grp', 'sp', 'tp')), parts along dimension 0
There are 2 independent parts, one for each index of `grp`. A program takes and returns all parts, laid end to end along the dimension named above; an argument that names none is the same for every part. Nothing has to cross between parts.
All inputs are finite; a program needn't handle non-finite values.
Results may differ from a plain program's by a relative error of at most 0.014.
The roundings to bfloat16 on the way count: a program that leaves them out, or rounds other values in their place, can miss the bound.
Values may be sent and summed in bfloat16 or wider, within the bound.
A program may use at most 64 MiB of HBM per device.

v0:
```python
import functools
import math

import jax
import jax.numpy as jnp
from jax import lax
from jax.experimental import pallas as pl
from jax.experimental.pallas import tpu as pltpu
from jax.sharding import PartitionSpec as P

HEAD = 128
QH_A = 16
WINDOW = 128
GRID_W = 64
THETA = 10000.0
NEGATIVE = -1e30
EPSILON = 1e-06
MESH = pl.DeviceIdType.MESH
F32 = jnp.float32
BF16 = jnp.bfloat16


def dot_nt(a, b):
    return lax.dot_general(a, b, (((1,), (1,)), ((), ())), preferred_element_type=F32)


def dot_tn(a, b):
    return lax.dot_general(a, b, (((0,), (0,)), ((), ())), preferred_element_type=F32)


def kernel(
    n, n_tp, rows, kvh, group, chunks,
    wq_hbm, wk_hbm, wv_hbm, gq_hbm, gk_hbm, gv_hbm, sink_ref, qgain_ref, kgain_ref, ww_hbm, gw_hbm,
    out_ref,
    qw, wkv, qraw, kraw, qg, kvbuf, ww, gw, cosine, sine, top, total, acc, attn, proj, pbuf, dbuf, sbuf, rbuf, own,
    lsem, gsend, grecv, hsend, hrecv, dsend, drecv, xsend, xrecv,
):
    me = lax.axis_index("sp")
    t = lax.axis_index("tp")
    core = lax.rem(t, 2)
    x = t // 2
    n_x = n_tp // 2
    partner = x * 2 + 1 - core
    out_rows = rows // n_tp
    width = ww.shape[1] // chunks
    span = group * rows
    has_left = me > 0
    has_right = me < n - 1

    loads = []

    def load(src, dst):
        copy = pltpu.make_async_copy(src, dst, lsem.at[len(loads)])
        copy.start()
        loads.append(copy)
        return copy

    def head_cols(h):
        return slice(h * HEAD, (h + 1) * HEAD)

    k_loads = [load(gk_hbm.at[:, head_cols(g)], kraw.at[g]) for g in range(kvh)]
    v_loads = [load(gv_hbm.at[:, head_cols(g)], kvbuf.at[me, g, 1]) for g in range(kvh)]
    w_loads = []
    for g in range(kvh):
        w_loads.append(load(wk_hbm.at[:, head_cols(g)], wkv.at[g, 0, WINDOW : WINDOW + rows]))
        w_loads.append(load(wv_hbm.at[:, head_cols(g)], wkv.at[g, 1, WINDOW : WINDOW + rows]))
    q_loads = []
    for g in range(kvh):
        for u in range(group):
            q_loads.append(load(gq_hbm.at[:, head_cols(g * group + u)], qraw.at[g, u * rows : (u + 1) * rows]))
    wq_loads = []
    for g in range(kvh):
        for u in range(group):
            wq_loads.append(load(wq_hbm.at[:, head_cols(g * group + u)], qw.at[g, u * rows : (u + 1) * rows]))
    ww_load = load(ww_hbm, ww)
    gw_load = load(gw_hbm, gw)

    barrier = pltpu.get_barrier_semaphore()

    def greet(device):
        pl.semaphore_signal(barrier, inc=1, device_id=device, device_id_type=MESH)

    @pl.when(has_left)
    def _():
        greet({"sp": me - 1})

    @pl.when(has_right)
    def _():
        greet({"sp": me + 1})

    greet({"tp": partner})
    for dx in range(1, n_x):
        greet({"tp": lax.rem(x + dx, n_x) * 2 + core})

    place = me * rows + lax.broadcasted_iota(jnp.int32, (rows, HEAD), 0)
    lane = lax.broadcasted_iota(jnp.int32, (rows, HEAD), 1)
    section = HEAD // 2
    half = section // 2
    frequency = jnp.exp(jnp.bitwise_and(lane, half - 1).astype(F32) * (-2.0 * math.log(THETA) / section))
    position = jnp.where(lane < section, place // GRID_W, lax.rem(place, GRID_W)).astype(F32)
    angle = position * frequency
    low = jnp.bitwise_and(lane, section - 1) < half
    cosine[...] = jnp.cos(angle)
    sine[...] = jnp.where(low, -jnp.sin(angle), jnp.sin(angle))

    def turn(values, gain):
        v = values.astype(F32)
        v = v * lax.rsqrt(jnp.mean(v * v, axis=1, keepdims=True) + EPSILON) * gain
        first = lax.broadcasted_iota(jnp.int32, v.shape, 1)
        other = jnp.where(
            jnp.bitwise_and(first, section - 1) < half,
            pltpu.roll(v, HEAD - half, 1),
            pltpu.roll(v, half, 1),
        )
        return (v * cosine[...] + other * sine[...]).astype(BF16)

    for g in range(kvh):
        k_loads[g].wait()
        kvbuf[me, g, 0] = turn(kraw[g], kgain_ref[...])
    for copy in v_loads:
        copy.wait()

    pl.semaphore_wait(barrier, has_left.astype(jnp.int32) + has_right.astype(jnp.int32) + n_x)

    def block_copy(source, g, direction):
        return pltpu.make_async_remote_copy(
            src_ref=kvbuf.at[source, g],
            dst_ref=kvbuf.at[source, g],
            send_sem=gsend.at[direction, source, g],
            recv_sem=grecv.at[source, g],
            device_id={"sp": me + 1 if direction == 0 else me - 1},
            device_id_type=MESH,
        )

    def halo_copy(direction):
        source = rows if direction == 0 else WINDOW
        target = 0 if direction == 0 else WINDOW + rows
        return pltpu.make_async_remote_copy(
            src_ref=wkv.at[:, :, source : source + WINDOW],
            dst_ref=wkv.at[:, :, target : target + WINDOW],
            send_sem=hsend.at[direction],
            recv_sem=hrecv.at[direction],
            device_id={"sp": me + 1 if direction == 0 else me - 1},
            device_id_type=MESH,
        )

    for g in range(kvh):
        @pl.when(has_right)
        def _():
            block_copy(me, g, 0).start()

        @pl.when(has_left)
        def _():
            block_copy(me, g, 1).start()

    for copy in w_loads:
        copy.wait()

    @pl.when(has_right)
    def _():
        halo_copy(0).start()

    @pl.when(has_left)
    def _():
        halo_copy(1).start()

    @pl.when(jnp.logical_not(has_left))
    def _():
        wkv[:, :, 0:WINDOW] = jnp.zeros((kvh, 2, WINDOW, HEAD), BF16)

    @pl.when(jnp.logical_not(has_right))
    def _():
        wkv[:, :, WINDOW + rows :] = jnp.zeros((kvh, 2, WINDOW, HEAD), BF16)

    for copy in q_loads:
        copy.wait()
    for g in range(kvh):
        for u in range(group):
            part = slice(u * rows, (u + 1) * rows)
            qg[g, part] = turn(qraw[g, part], qgain_ref[...])

    scale = HEAD ** (-0.5)

    def absorb(source, g, first=False):
        scores = dot_nt(kvbuf[source, g, 0], qg[g]) * scale
        block_top = jnp.max(scores, axis=0, keepdims=True)
        if first:
            raised = jnp.exp(scores - block_top)
            top[g] = block_top
            total[g] = jnp.sum(raised, axis=0, keepdims=True)
            acc[g] = dot_tn(kvbuf[source, g, 1], raised.astype(BF16))
        else:
            before = top[g]
            new_top = jnp.maximum(before, block_top)
            fading = jnp.exp(before - new_top)
            raised = jnp.exp(scores - new_top)
            top[g] = new_top
            total[g] = total[g] * fading + jnp.sum(raised, axis=0, keepdims=True)
            acc[g] = acc[g] * fading + dot_tn(kvbuf[source, g, 1], raised.astype(BF16))

    for g in range(kvh):
        absorb(me, g, True)

    def relay(d):
        for g in range(kvh):
            @pl.when(me - d >= 0)
            def _():
                block_copy(me - d, g, 0).wait_recv()

                @pl.when(has_right)
                def _():
                    block_copy(me - d, g, 0).start()

            @pl.when(me + d < n)
            def _():
                block_copy(me + d, g, 1).wait_recv()

                @pl.when(has_left)
                def _():
                    block_copy(me + d, g, 1).start()

            @pl.when(me - d >= 0)
            def _():
                absorb(me - d, g)

            @pl.when(me + d < n)
            def _():
                absorb(me + d, g)

    def put_heads(base, g, value):
        turned = jnp.transpose(value).astype(BF16)
        for u in range(group):
            attn[:, base + (g * group + u) * HEAD : base + (g * group + u + 1) * HEAD] = turned[u * rows : (u + 1) * rows]

    heads_width = kvh * group * HEAD

    def windowed():
        for copy in wq_loads:
            copy.wait()

        @pl.when(has_left)
        def _():
            halo_copy(0).wait_recv()

        @pl.when(has_right)
        def _():
            halo_copy(1).wait_recv()

        padded = rows + 2 * WINDOW
        key_at = lax.broadcasted_iota(jnp.int32, (padded, span), 0) - WINDOW
        column = lax.broadcasted_iota(jnp.int32, (padded, span), 1)
        distance = jnp.abs(key_at - lax.rem(column, rows))
        key_place = me * rows + key_at
        inside = (distance <= WINDOW) & (key_place >= 0) & (key_place < n * rows)
        far = distance.astype(F32)
        member = lax.broadcasted_iota(jnp.int32, (1, span), 1) // rows
        for g in range(kvh):
            head = (t * (kvh * group) + g * group + 1 + member).astype(F32)
            slope = jnp.exp2(head * (-8.0 / QH_A))
            sink = jnp.zeros((1, span), F32)
            for u in range(group):
                sink = jnp.where(member == u, sink_ref[g * group + u], sink)
            scores = dot_nt(wkv[g, 0], qw[g]) * scale
            scores = jnp.where(inside, scores - slope * far, NEGATIVE)
            highest = jnp.maximum(jnp.max(scores, axis=0, keepdims=True), sink)
            raised = jnp.exp(scores - highest)
            bottom = jnp.sum(raised, axis=0, keepdims=True) + jnp.exp(sink - highest)
            weights = (raised * (1.0 / bottom)).astype(BF16)
            put_heads(0, g, dot_tn(wkv[g, 1], weights))
        ww_load.wait()
        for j in range(chunks):
            cols = slice(j * width, (j + 1) * width)
            proj[:, cols] = jnp.dot(attn[:, :heads_width], ww[:, cols], preferred_element_type=F32)

    if n > 1:
        relay(1)
    windowed()
    if n <= 4:
        for d in range(2, n):
            relay(d)
    else:
        def relay_step(d, carry):
            relay(d)
            return carry

        lax.fori_loop(2, n, relay_step, 0)

    for g in range(kvh):
        put_heads(heads_width, g, acc[g] * (1.0 / total[g]))
    gw_load.wait()

    def pair_copy(j):
        return pltpu.make_async_remote_copy(
            src_ref=pbuf.at[j, 1 - core],
            dst_ref=dbuf.at[j],
            send_sem=dsend.at[j],
            recv_sem=drecv.at[j],
            device_id={"tp": partner},
            device_id_type=MESH,
        )

    def cross_copy(j, dx):
        return pltpu.make_async_remote_copy(
            src_ref=sbuf.at[j, dx - 1],
            dst_ref=rbuf.at[j, dx - 1],
            send_sem=xsend.at[j, dx - 1],
            recv_sem=xrecv.at[j, dx - 1],
            device_id={"tp": lax.rem(x + dx, n_x) * 2 + core},
            device_id_type=MESH,
        )

    def pass_on(j):
        pair_copy(j).wait_recv()
        for dx in range(1, n_x):
            other = lax.rem(x + dx, n_x)
            sbuf[j, dx - 1] = (pbuf[j, core, other].astype(F32) + dbuf[j, other].astype(F32)).astype(BF16)
            cross_copy(j, dx).start()
        own[j] = pbuf[j, core, x].astype(F32) + dbuf[j, x].astype(F32)

    for j in range(chunks):
        cols = slice(j * width, (j + 1) * width)
        part = proj[:, cols] + jnp.dot(attn[:, heads_width:], gw[:, cols], preferred_element_type=F32)
        for b in range(n_tp):
            pbuf[j, b % 2, b // 2] = part[b * out_rows : (b + 1) * out_rows].astype(BF16)
        pair_copy(j).start()
        if j >= 1:
            pass_on(j - 1)
    pass_on(chunks - 1)
    for j in range(chunks):
        value = own[j]
        for dx in range(1, n_x):
            cross_copy(j, dx).wait_recv()
            value = value + rbuf[j, dx - 1].astype(F32)
        out_ref[:, j * width : (j + 1) * width] = value.astype(BF16)

    for j in range(chunks):
        pair_copy(j).wait_send()
        for dx in range(1, n_x):
            cross_copy(j, dx).wait_send()

    @pl.when(has_right)
    def _():
        halo_copy(0).wait_send()

    @pl.when(has_left)
    def _():
        halo_copy(1).wait_send()

    def drain(source, carry):
        for g in range(kvh):
            @pl.when(has_right & (source <= me))
            def _():
                block_copy(source, g, 0).wait_send()

            @pl.when(has_left & (source >= me))
            def _():
                block_copy(source, g, 1).wait_send()

        return carry

    lax.fori_loop(0, n, drain, 0)


def solution(mesh):
    n, n_tp = mesh.shape["sp"], mesh.shape["tp"]

    def per_device(wq, wk, wv, gq, gk, gv, sink, qgain, kgain, ww, gw):
        rows = wq.shape[0]
        kvh = wk.shape[1] // HEAD
        group = wq.shape[1] // wk.shape[1]
        model = ww.shape[1]
        chunks = 8
        width = model // chunks
        n_x = n_tp // 2
        out_rows = rows // n_tp
        heads_width = kvh * group * HEAD
        span = group * rows
        any_spec = pl.BlockSpec(memory_space=pl.ANY)
        vmem = pl.BlockSpec(memory_space=pltpu.VMEM)
        smem = pl.BlockSpec(memory_space=pltpu.SMEM)
        cross = max(n_x - 1, 1)
        return pl.pallas_call(
            functools.partial(kernel, n, n_tp, rows, kvh, group, chunks),
            out_shape=jax.ShapeDtypeStruct((out_rows, model), BF16),
            in_specs=[any_spec] * 6 + [smem, vmem, vmem, any_spec, any_spec],
            out_specs=vmem,
            scratch_shapes=[
                pltpu.VMEM((kvh, span, HEAD), BF16),
                pltpu.VMEM((kvh, 2, rows + 2 * WINDOW, HEAD), BF16),
                pltpu.VMEM((kvh, span, HEAD), BF16),
                pltpu.VMEM((kvh, rows, HEAD), BF16),
                pltpu.VMEM((kvh, span, HEAD), BF16),
                pltpu.VMEM((n, kvh, 2, rows, HEAD), BF16),
                pltpu.VMEM(ww.shape, BF16),
                pltpu.VMEM(gw.shape, BF16),
                pltpu.VMEM((rows, HEAD), F32),
                pltpu.VMEM((rows, HEAD), F32),
                pltpu.VMEM((kvh, 1, span), F32),
                pltpu.VMEM((kvh, 1, span), F32),
                pltpu.VMEM((kvh, HEAD, span), F32),
                pltpu.VMEM((rows, 2 * heads_width), BF16),
                pltpu.VMEM((rows, model), F32),
                pltpu.VMEM((chunks, 2, n_x, out_rows, width), BF16),
                pltpu.VMEM((chunks, n_x, out_rows, width), BF16),
                pltpu.VMEM((chunks, cross, out_rows, width), BF16),
                pltpu.VMEM((chunks, cross, out_rows, width), BF16),
                pltpu.VMEM((chunks, out_rows, width), F32),
                pltpu.SemaphoreType.DMA((4 * kvh + 2 * kvh * group + 2,)),
                pltpu.SemaphoreType.DMA((2, n, kvh)),
                pltpu.SemaphoreType.DMA((n, kvh)),
                pltpu.SemaphoreType.DMA((2,)),
                pltpu.SemaphoreType.DMA((2,)),
                pltpu.SemaphoreType.DMA((chunks,)),
                pltpu.SemaphoreType.DMA((chunks,)),
                pltpu.SemaphoreType.DMA((chunks, cross)),
                pltpu.SemaphoreType.DMA((chunks, cross)),
            ],
            compiler_params=pltpu.CompilerParams(
                collective_id=0, has_side_effects=True, vmem_limit_bytes=60 * 1024 * 1024
            ),
            name="hybrid",
        )(wq, wk, wv, gq, gk, gv, sink, qgain.reshape(1, HEAD), kgain.reshape(1, HEAD), ww, gw)

    return jax.shard_map(
        per_device,
        mesh=mesh,
        in_specs=(P(("grp", "sp"), "tp"),) * 6 + (P("tp"), P(), P(), P("tp", None), P("tp", None)),
        out_specs=P(("grp", "sp", "tp"), None),
        check_vma=False,
    )
```

profile of v0, /device:TPU:0, one launch (start us, length us, event | category | flops | bytes accessed | tf_op | source)
XLA Modules:
  0.0 51.6 jit_solution(1351477151606443794)
XLA Ops:
  0.0 49.6 %hybrid.1 = bf16[80,4096]{1,0:T(8,128)(2,1)} custom-call(bf16[320,512]{1,0:T(8,128)(2,1)} %wq_hbm.1, bf16[320,256]{1,0:T(8,128)(2,1)} %wk_hbm.1, bf16[320,256]{1,0:T(8,128)(2,1)} %wv_hbm.1, bf16[320,512]{1,0:T(8,128)(2,1)} %gq_hbm.1, bf16[320,256]{1,0:T(8,128)(2,1)} %gk_hbm.1, bf16[320,256]{1,0:T(8,128)(2,1)} %gv_hbm.1, f32[4]{0:T(128)} %sink_ref.1, ...), custom_call_target="tpu_custom_call" | custom-call | tf_op jit(solution)/shard_map/hybrid/pallas_call | solution.py:382
  49.6 2.0 %copy.13 = bf16[80,4096]{1,0:T(8,128)(2,1)} copy(bf16[80,4096]{1,0:T(8,128)(2,1)} %hybrid.1) | data formatting | bytes 1310720
where the time goes:
time: 51.7 us; the launch traced here: 51.6 us
  Pallas kernels  49.6 us (96%)
  local copies, waits for them, and re-layouts  1.97 us (4%)
    pallas_call x1, Pallas kernels, per_device(): pl.pallas_call(functools.partial(kernel, n, n_tp, rows, kvh, group, chunk...  49.6 us
    unnamed x1, local copies, waits for them, and re-layouts  1.97 us

commit v1 on v0

--- a/solution.py
+++ b/solution.py
@@ -30,9 +30,9 @@
 
 def kernel(
     n, n_tp, rows, kvh, group, chunks,
-    wq_hbm, wk_hbm, wv_hbm, gq_hbm, gk_hbm, gv_hbm, sink_ref, qgain_ref, kgain_ref, ww_hbm, gw_hbm,
+    wq_hbm, wk_hbm, wv_hbm, gq_hbm, gk_hbm, gv_hbm, sink_hbm, qgain_hbm, kgain_hbm, ww_hbm, gw_hbm,
     out_ref,
-    qw, wkv, qraw, kraw, qg, kvbuf, ww, gw, cosine, sine, top, total, acc, attn, proj, pbuf, dbuf, sbuf, rbuf, own,
+    sink_ref, qgain_ref, kgain_ref, qw, wkv, qraw, kraw, qg, kvbuf, ww, gw, cosine, sine, top, total, acc, attn, proj, pbuf, dbuf, sbuf, rbuf, own,
     lsem, gsend, grecv, hsend, hrecv, dsend, drecv, xsend, xrecv,
 ):
     me = lax.axis_index("sp")
@@ -47,6 +47,23 @@
     has_left = me > 0
     has_right = me < n - 1
 
+    barrier = pltpu.get_barrier_semaphore()
+
+    def greet(device):
+        pl.semaphore_signal(barrier, inc=1, device_id=device, device_id_type=MESH)
+
+    @pl.when(has_left)
+    def _():
+        greet({"sp": me - 1})
+
+    @pl.when(has_right)
+    def _():
+        greet({"sp": me + 1})
+
+    greet({"tp": partner})
+    for dx in range(1, n_x):
+        greet({"tp": lax.rem(x + dx, n_x) * 2 + core})
+
     loads = []
 
     def load(src, dst):
@@ -58,8 +75,11 @@
     def head_cols(h):
         return slice(h * HEAD, (h + 1) * HEAD)
 
+    v_loads = [load(gv_hbm.at[:, head_cols(g)], kvbuf.at[me, g, 1]) for g in range(kvh)]
     k_loads = [load(gk_hbm.at[:, head_cols(g)], kraw.at[g]) for g in range(kvh)]
-    v_loads = [load(gv_hbm.at[:, head_cols(g)], kvbuf.at[me, g, 1]) for g in range(kvh)]
+    kgain_load = load(kgain_hbm, kgain_ref)
+    qgain_load = load(qgain_hbm, qgain_ref)
+    sink_load = load(sink_hbm, sink_ref)
     w_loads = []
     for g in range(kvh):
         w_loads.append(load(wk_hbm.at[:, head_cols(g)], wkv.at[g, 0, WINDOW : WINDOW + rows]))
@@ -75,33 +95,36 @@
     ww_load = load(ww_hbm, ww)
     gw_load = load(gw_hbm, gw)
 
-    barrier = pltpu.get_barrier_semaphore()
-
-    def greet(device):
-        pl.semaphore_signal(barrier, inc=1, device_id=device, device_id_type=MESH)
-
-    @pl.when(has_left)
-    def _():
-        greet({"sp": me - 1})
-
-    @pl.when(has_right)
-    def _():
-        greet({"sp": me + 1})
-
-    greet({"tp": partner})
-    for dx in range(1, n_x):
-        greet({"tp": lax.rem(x + dx, n_x) * 2 + core})
-
-    place = me * rows + lax.broadcasted_iota(jnp.int32, (rows, HEAD), 0)
-    lane = lax.broadcasted_iota(jnp.int32, (rows, HEAD), 1)
     section = HEAD // 2
     half = section // 2
-    frequency = jnp.exp(jnp.bitwise_and(lane, half - 1).astype(F32) * (-2.0 * math.log(THETA) / section))
-    position = jnp.where(lane < section, place // GRID_W, lax.rem(place, GRID_W)).astype(F32)
-    angle = position * frequency
-    low = jnp.bitwise_and(lane, section - 1) < half
-    cosine[...] = jnp.cos(angle)
-    sine[...] = jnp.where(low, -jnp.sin(angle), jnp.sin(angle))
+
+    def angles(row_place, column_place, shape):
+        lane = lax.broadcasted_iota(jnp.int32, shape, 1)
+        frequency = jnp.exp(jnp.bitwise_and(lane, half - 1).astype(F32) * (-2.0 * math.log(THETA) / section))
+        return jnp.where(lane < section, row_place, column_place).astype(F32) * frequency
+
+    def signed_sine(angle):
+        low = jnp.bitwise_and(lax.broadcasted_iota(jnp.int32, angle.shape, 1), section - 1) < half
+        return jnp.where(low, -jnp.sin(angle), jnp.sin(angle))
+
+    def make_tables():
+        if rows % GRID_W:
+            place = me * rows + lax.broadcasted_iota(jnp.int32, (rows, HEAD), 0)
+            angle = angles(place // GRID_W, lax.rem(place, GRID_W), (rows, HEAD))
+            cosine[...] = jnp.cos(angle)
+            sine[...] = signed_sine(angle)
+            return
+        lines = rows // GRID_W
+        shape = (-(-lines // 8) * 8, HEAD)
+        line = me * lines + lax.broadcasted_iota(jnp.int32, shape, 0)
+        row_angle = angles(line, line, shape)
+        column = lax.broadcasted_iota(jnp.int32, (GRID_W, HEAD), 0)
+        column_angle = angles(column, column, (GRID_W, HEAD))
+        by_row = lax.broadcasted_iota(jnp.int32, (GRID_W, HEAD), 1) < section
+        for table, of in ((cosine, jnp.cos), (sine, signed_sine)):
+            per_row, per_column = of(row_angle), of(column_angle)
+            for r in range(lines):
+                table[r * GRID_W : (r + 1) * GRID_W] = jnp.where(by_row, per_row[r : r + 1], per_column)
 
     def turn(values, gain):
         v = values.astype(F32)
@@ -114,23 +137,24 @@
         )
         return (v * cosine[...] + other * sine[...]).astype(BF16)
 
-    for g in range(kvh):
-        k_loads[g].wait()
-        kvbuf[me, g, 0] = turn(kraw[g], kgain_ref[...])
-    for copy in v_loads:
-        copy.wait()
-
-    pl.semaphore_wait(barrier, has_left.astype(jnp.int32) + has_right.astype(jnp.int32) + n_x)
-
-    def block_copy(source, g, direction):
+    def block_copy(source, g, part, direction):
         return pltpu.make_async_remote_copy(
-            src_ref=kvbuf.at[source, g],
-            dst_ref=kvbuf.at[source, g],
-            send_sem=gsend.at[direction, source, g],
-            recv_sem=grecv.at[source, g],
+            src_ref=kvbuf.at[source, g, part],
+            dst_ref=kvbuf.at[source, g, part],
+            send_sem=gsend.at[direction, source, g, part],
+            recv_sem=grecv.at[source, g, part],
             device_id={"sp": me + 1 if direction == 0 else me - 1},
             device_id_type=MESH,
         )
+
+    def spread(g, part):
+        @pl.when(has_right)
+        def _():
+            block_copy(me, g, part, 0).start()
+
+        @pl.when(has_left)
+        def _():
+            block_copy(me, g, part, 1).start()
 
     def halo_copy(direction):
         source = rows if direction == 0 else WINDOW
@@ -144,14 +168,18 @@
             device_id_type=MESH,
         )
 
-    for g in range(kvh):
-        @pl.when(has_right)
-        def _():
-            block_copy(me, g, 0).start()
-
-        @pl.when(has_left)
-        def _():
-            block_copy(me, g, 1).start()
+    for copy in v_loads:
+        copy.wait()
+    pl.semaphore_wait(barrier, has_left.astype(jnp.int32) + has_right.astype(jnp.int32) + n_x)
+    for g in range(kvh):
+        spread(g, 1)
+
+    make_tables()
+    kgain_load.wait()
+    for g in range(kvh):
+        k_loads[g].wait()
+        kvbuf[me, g, 0] = turn(kraw[g], kgain_ref[...])
+        spread(g, 0)
 
     for copy in w_loads:
         copy.wait()
@@ -172,6 +200,7 @@
     def _():
         wkv[:, :, WINDOW + rows :] = jnp.zeros((kvh, 2, WINDOW, HEAD), BF16)
 
+    qgain_load.wait()
     for copy in q_loads:
         copy.wait()
     for g in range(kvh):
@@ -202,30 +231,32 @@
         absorb(me, g, True)
 
     def relay(d):
-        for g in range(kvh):
-            @pl.when(me - d >= 0)
-            def _():
-                block_copy(me - d, g, 0).wait_recv()
-
-                @pl.when(has_right)
+        for part in (1, 0):
+            for g in range(kvh):
+                @pl.when(me - d >= 0)
                 def _():
-                    block_copy(me - d, g, 0).start()
-
-            @pl.when(me + d < n)
-            def _():
-                block_copy(me + d, g, 1).wait_recv()
-
-                @pl.when(has_left)
+                    block_copy(me - d, g, part, 0).wait_recv()
+
+                    @pl.when(has_right)
+                    def _():
+                        block_copy(me - d, g, part, 0).start()
+
+                @pl.when(me + d < n)
                 def _():
-                    block_copy(me + d, g, 1).start()
-
-            @pl.when(me - d >= 0)
-            def _():
-                absorb(me - d, g)
-
-            @pl.when(me + d < n)
-            def _():
-                absorb(me + d, g)
+                    block_copy(me + d, g, part, 1).wait_recv()
+
+                    @pl.when(has_left)
+                    def _():
+                        block_copy(me + d, g, part, 1).start()
+
+                if part == 0:
+                    @pl.when(me - d >= 0)
+                    def _():
+                        absorb(me - d, g)
+
+                    @pl.when(me + d < n)
+                    def _():
+                        absorb(me + d, g)
 
     def put_heads(base, g, value):
         turned = jnp.transpose(value).astype(BF16)
@@ -235,6 +266,7 @@
     heads_width = kvh * group * HEAD
 
     def windowed():
+        sink_load.wait()
         for copy in wq_loads:
             copy.wait()
 
@@ -348,13 +380,14 @@
 
     def drain(source, carry):
         for g in range(kvh):
-            @pl.when(has_right & (source <= me))
-            def _():
-                block_copy(source, g, 0).wait_send()
-
-            @pl.when(has_left & (source >= me))
-            def _():
-                block_copy(source, g, 1).wait_send()
+            for part in range(2):
+                @pl.when(has_right & (source <= me))
+                def _():
+                    block_copy(source, g, part, 0).wait_send()
+
+                @pl.when(has_left & (source >= me))
+                def _():
+                    block_copy(source, g, part, 1).wait_send()
 
         return carry
 
@@ -377,14 +410,16 @@
         span = group * rows
         any_spec = pl.BlockSpec(memory_space=pl.ANY)
         vmem = pl.BlockSpec(memory_space=pltpu.VMEM)
-        smem = pl.BlockSpec(memory_space=pltpu.SMEM)
         cross = max(n_x - 1, 1)
         return pl.pallas_call(
             functools.partial(kernel, n, n_tp, rows, kvh, group, chunks),
-            out_shape=jax.ShapeDtypeStruct((out_rows, model), BF16),
-            in_specs=[any_spec] * 6 + [smem, vmem, vmem, any_spec, any_spec],
+            out_shape=pltpu.VMEM((out_rows, model), BF16),
+            in_specs=[any_spec] * 11,
             out_specs=vmem,
             scratch_shapes=[
+                pltpu.SMEM(sink.shape, F32),
+                pltpu.VMEM((1, HEAD), F32),
+                pltpu.VMEM((1, HEAD), F32),
                 pltpu.VMEM((kvh, span, HEAD), BF16),
                 pltpu.VMEM((kvh, 2, rows + 2 * WINDOW, HEAD), BF16),
                 pltpu.VMEM((kvh, span, HEAD), BF16),
@@ -405,9 +440,9 @@
                 pltpu.VMEM((chunks, cross, out_rows, width), BF16),
                 pltpu.VMEM((chunks, cross, out_rows, width), BF16),
                 pltpu.VMEM((chunks, out_rows, width), F32),
-                pltpu.SemaphoreType.DMA((4 * kvh + 2 * kvh * group + 2,)),
-                pltpu.SemaphoreType.DMA((2, n, kvh)),
-                pltpu.SemaphoreType.DMA((n, kvh)),
+                pltpu.SemaphoreType.DMA((4 * kvh + 2 * kvh * group + 5,)),
+                pltpu.SemaphoreType.DMA((2, n, kvh, 2)),
+                pltpu.SemaphoreType.DMA((n, kvh, 2)),
                 pltpu.SemaphoreType.DMA((2,)),
                 pltpu.SemaphoreType.DMA((2,)),
                 pltpu.SemaphoreType.DMA((chunks,)),

time: 51.7 us -> 49.3 us (0.954)
  Pallas kernels: 49.6 us -> 48.3 us
  local copies, waits for them, and re-layouts: 1.97 us -> 0.84 us
    pallas_call x1, Pallas kernels: 49.6 us -> 48.3 us  [per_device(): pl.pallas_call(functools.partial(kernel, n, n_tp, rows, kvh, group, chunk...]
    unnamed x1, local copies, waits for them, and re-layouts: 1.97 us -> 0.84 us
where the time goes in v1:
time: 49.3 us; the launch traced here: 49.1 us
  Pallas kernels  48.3 us (98%)
  local copies, waits for them, and re-layouts  0.84 us (2%)
    pallas_call x1, Pallas kernels, per_device(): pl.pallas_call(functools.partial(kernel, n, n_tp, rows, kvh, group, chunk...  48.3 us

profile of v1, /device:TPU:0, one launch (start us, length us, event | category | flops | bytes accessed | tf_op | source)
XLA Modules:
  0.0 49.1 jit_solution(12403785321289459999)
XLA Ops:
  0.0 48.3 %hybrid.1 = bf16[80,4096]{1,0:T(8,128)(2,1)S(1)} custom-call(bf16[320,512]{1,0:T(8,128)(2,1)} %wq_hbm.1, bf16[320,256]{1,0:T(8,128)(2,1)} %wk_hbm.1, bf16[320,256]{1,0:T(8,128)(2,1)} %wv_hbm.1, bf16[320,512]{1,0:T(8,128)(2,1)} %gq_hbm.1, bf16[320,256]{1,0:T(8,128)(2,1)} %gk_hbm.1, bf16[320,256]{1,0:T(8,128)(2,1)} %gv_hbm.1, f32[4]{0:T(128)} %sink_hbm.1, ...), custom_call_target="tpu_custom_call" | custom-call | tf_op jit(solution)/shard_map/hybrid/pallas_call | solution.py:414
  48.3 0.8 %copy.13 = bf16[80,4096]{1,0:T(8,128)(2,1)} copy(bf16[80,4096]{1,0:T(8,128)(2,1)S(1)} %hybrid.1) | data formatting | bytes 1310720

commit v2 on v1

--- a/solution.py
+++ b/solution.py
@@ -15,6 +15,7 @@
 THETA = 10000.0
 NEGATIVE = -1e30
 EPSILON = 1e-06
+LAG = 1
 MESH = pl.DeviceIdType.MESH
 F32 = jnp.float32
 BF16 = jnp.bfloat16
@@ -29,11 +30,11 @@
 
 
 def kernel(
-    n, n_tp, rows, kvh, group, chunks,
+    n, n_tp, rows, kvh, group, chunks, detours,
     wq_hbm, wk_hbm, wv_hbm, gq_hbm, gk_hbm, gv_hbm, sink_hbm, qgain_hbm, kgain_hbm, ww_hbm, gw_hbm,
     out_ref,
-    sink_ref, qgain_ref, kgain_ref, qw, wkv, qraw, kraw, qg, kvbuf, ww, gw, cosine, sine, top, total, acc, attn, proj, pbuf, dbuf, sbuf, rbuf, own,
-    lsem, gsend, grecv, hsend, hrecv, dsend, drecv, xsend, xrecv,
+    sink_ref, qgain_ref, kgain_ref, qw, wkv, qraw, kraw, qg, kvbuf, ww, gw, cosine, sine, top, total, acc, attn, proj, pbuf, dbuf, sbuf, rbuf, own, detour,
+    lsem, gsend, grecv, hsend, hrecv, dsend, drecv, xsend, xrecv, rsend, rrecv,
 ):
     me = lax.axis_index("sp")
     t = lax.axis_index("tp")
@@ -46,6 +47,10 @@
     span = group * rows
     has_left = me > 0
     has_right = me < n - 1
+    at_end = jnp.logical_not(has_left & has_right)
+    beside_end = (me == 1) | (me == n - 2)
+    inner = jnp.where(me == 0, 1, n - 2)
+    outer = jnp.where(me == 1, 0, n - 1)
 
     barrier = pltpu.get_barrier_semaphore()
 
@@ -63,6 +68,16 @@
     greet({"tp": partner})
     for dx in range(1, n_x):
         greet({"tp": lax.rem(x + dx, n_x) * 2 + core})
+    if detours:
+        across = lax.rem(x + 1, n_x) * 2 + core
+
+        @pl.when(at_end)
+        def _():
+            greet({"sp": inner, "tp": across})
+
+        @pl.when(beside_end)
+        def _():
+            greet({"sp": outer, "tp": across})
 
     loads = []
 
@@ -170,7 +185,10 @@
 
     for copy in v_loads:
         copy.wait()
-    pl.semaphore_wait(barrier, has_left.astype(jnp.int32) + has_right.astype(jnp.int32) + n_x)
+    greeted = has_left.astype(jnp.int32) + has_right.astype(jnp.int32) + n_x
+    if detours:
+        greeted = greeted + at_end.astype(jnp.int32) + beside_end.astype(jnp.int32)
+    pl.semaphore_wait(barrier, greeted)
     for g in range(kvh):
         spread(g, 1)
 
@@ -341,12 +359,41 @@
             device_id_type=MESH,
         )
 
+    def detour_copy(j):
+        return pltpu.make_async_remote_copy(
+            src_ref=sbuf.at[j, 0],
+            dst_ref=detour.at[detours.index(j)],
+            send_sem=xsend.at[j, 0],
+            recv_sem=rrecv.at[detours.index(j)],
+            device_id={"sp": inner, "tp": across},
+            device_id_type=MESH,
+        )
+
+    def detour_end_copy(j):
+        return pltpu.make_async_remote_copy(
+            src_ref=detour.at[detours.index(j)],
+            dst_ref=rbuf.at[j, 0],
+            send_sem=rsend.at[detours.index(j)],
+            recv_sem=xrecv.at[j, 0],
+            device_id={"sp": outer},
+            device_id_type=MESH,
+        )
+
     def pass_on(j):
         pair_copy(j).wait_recv()
         for dx in range(1, n_x):
             other = lax.rem(x + dx, n_x)
             sbuf[j, dx - 1] = (pbuf[j, core, other].astype(F32) + dbuf[j, other].astype(F32)).astype(BF16)
-            cross_copy(j, dx).start()
+            if j in detours:
+                @pl.when(at_end)
+                def _():
+                    detour_copy(j).start()
+
+                @pl.when(jnp.logical_not(at_end))
+                def _():
+                    cross_copy(j, dx).start()
+            else:
+                cross_copy(j, dx).start()
         own[j] = pbuf[j, core, x].astype(F32) + dbuf[j, x].astype(F32)
 
     for j in range(chunks):
@@ -355,9 +402,16 @@
         for b in range(n_tp):
             pbuf[j, b % 2, b // 2] = part[b * out_rows : (b + 1) * out_rows].astype(BF16)
         pair_copy(j).start()
-        if j >= 1:
-            pass_on(j - 1)
-    pass_on(chunks - 1)
+        if j >= LAG:
+            pass_on(j - LAG)
+    for j in range(chunks - LAG, chunks):
+        pass_on(j)
+    for j in detours:
+        @pl.when(beside_end)
+        def _():
+            detour_copy(j).wait_recv()
+            detour_end_copy(j).start()
+
     for j in range(chunks):
         value = own[j]
         for dx in range(1, n_x):
@@ -369,6 +423,10 @@
         pair_copy(j).wait_send()
         for dx in range(1, n_x):
             cross_copy(j, dx).wait_send()
+    for j in detours:
+        @pl.when(beside_end)
+        def _():
+            detour_end_copy(j).wait_send()
 
     @pl.when(has_right)
     def _():
@@ -411,8 +469,9 @@
         any_spec = pl.BlockSpec(memory_space=pl.ANY)
         vmem = pl.BlockSpec(memory_space=pltpu.VMEM)
         cross = max(n_x - 1, 1)
+        detours = (1, 3) if n >= 4 and n_x == 2 else ()
         return pl.pallas_call(
-            functools.partial(kernel, n, n_tp, rows, kvh, group, chunks),
+            functools.partial(kernel, n, n_tp, rows, kvh, group, chunks, detours),
             out_shape=pltpu.VMEM((out_rows, model), BF16),
             in_specs=[any_spec] * 11,
             out_specs=vmem,
@@ -440,6 +499,7 @@
                 pltpu.VMEM((chunks, cross, out_rows, width), BF16),
                 pltpu.VMEM((chunks, cross, out_rows, width), BF16),
                 pltpu.VMEM((chunks, out_rows, width), F32),
+                pltpu.VMEM((max(len(detours), 1), out_rows, width), BF16),
                 pltpu.SemaphoreType.DMA((4 * kvh + 2 * kvh * group + 5,)),
                 pltpu.SemaphoreType.DMA((2, n, kvh, 2)),
                 pltpu.SemaphoreType.DMA((n, kvh, 2)),
@@ -449,6 +509,8 @@
                 pltpu.SemaphoreType.DMA((chunks,)),
                 pltpu.SemaphoreType.DMA((chunks, cross)),
                 pltpu.SemaphoreType.DMA((chunks, cross)),
+                pltpu.SemaphoreType.DMA((max(len(detours), 1),)),
+                pltpu.SemaphoreType.DMA((max(len(detours), 1),)),
             ],
             compiler_params=pltpu.CompilerParams(
                 collective_id=0, has_side_effects=True, vmem_limit_bytes=60 * 1024 * 1024

time: 49.3 us -> 46.3 us (0.939)
  Pallas kernels: 48.3 us -> 45.3 us
    pallas_call x1, Pallas kernels: 48.3 us -> 45.3 us  [per_device(): pl.pallas_call(functools.partial(kernel, n, n_tp, rows, kvh, group, chunk...]
where the time goes in v2:
time: 46.3 us; the launch traced here: 46.2 us
  Pallas kernels  45.3 us (98%)
  local copies, waits for them, and re-layouts  0.84 us (2%)
    pallas_call x1, Pallas kernels, per_device(): pl.pallas_call(functools.partial(kernel, n, n_tp, rows, kvh, group, chunk...  45.3 us

profile of v2, /device:TPU:0, one launch (start us, length us, event | category | flops | bytes accessed | tf_op | source)
XLA Modules:
  0.0 46.2 jit_solution(1997451405224318556)
XLA Ops:
  0.0 45.3 %hybrid.1 = bf16[80,4096]{1,0:T(8,128)(2,1)S(1)} custom-call(bf16[320,512]{1,0:T(8,128)(2,1)} %wq_hbm.1, bf16[320,256]{1,0:T(8,128)(2,1)} %wk_hbm.1, bf16[320,256]{1,0:T(8,128)(2,1)} %wv_hbm.1, bf16[320,512]{1,0:T(8,128)(2,1)} %gq_hbm.1, bf16[320,256]{1,0:T(8,128)(2,1)} %gk_hbm.1, bf16[320,256]{1,0:T(8,128)(2,1)} %gv_hbm.1, f32[4]{0:T(128)} %sink_hbm.1, ...), custom_call_target="tpu_custom_call" | custom-call | tf_op jit(solution)/shard_map/hybrid/pallas_call | solution.py:473
  45.3 0.8 %copy.13 = bf16[80,4096]{1,0:T(8,128)(2,1)} copy(bf16[80,4096]{1,0:T(8,128)(2,1)S(1)} %hybrid.1) | data formatting | bytes 1310720

commit v3 on v2

--- a/solution.py
+++ b/solution.py
@@ -13,9 +13,10 @@
 WINDOW = 128
 GRID_W = 64
 THETA = 10000.0
-NEGATIVE = -1e30
+AWAY = 1e30
 EPSILON = 1e-06
-LAG = 1
+DIRECT = 128
+LEND = True
 MESH = pl.DeviceIdType.MESH
 F32 = jnp.float32
 BF16 = jnp.bfloat16
@@ -30,11 +31,11 @@
 
 
 def kernel(
-    n, n_tp, rows, kvh, group, chunks, detours,
+    n, n_tp, rows, kvh, group, cuts, direct, detours, lend,
     wq_hbm, wk_hbm, wv_hbm, gq_hbm, gk_hbm, gv_hbm, sink_hbm, qgain_hbm, kgain_hbm, ww_hbm, gw_hbm,
     out_ref,
-    sink_ref, qgain_ref, kgain_ref, qw, wkv, qraw, kraw, qg, kvbuf, ww, gw, cosine, sine, top, total, acc, attn, proj, pbuf, dbuf, sbuf, rbuf, own, detour,
-    lsem, gsend, grecv, hsend, hrecv, dsend, drecv, xsend, xrecv, rsend, rrecv,
+    sink_ref, qgain_ref, kgain_ref, qw, wkv, qraw, kraw, qg, kvbuf, ww, gw, cosine, sine, top, total, acc, attn, proj, pbuf, dbuf, sbuf, rbuf, own, detour, lent, lent_sums, xbuf, far,
+    lsem, gsend, grecv, hsend, hrecv, dsend, drecv, xsend, xrecv, rsend, rrecv, lsend, lrecv, usend, urecv,
 ):
     me = lax.axis_index("sp")
     t = lax.axis_index("tp")
@@ -43,14 +44,18 @@
     n_x = n_tp // 2
     partner = x * 2 + 1 - core
     out_rows = rows // n_tp
-    width = ww.shape[1] // chunks
+    chunks = len(cuts)
     span = group * rows
+    spans = [slice(begin, end) for begin, end in cuts]
+    sizes = [slice(0, end - begin) for begin, end in cuts]
     has_left = me > 0
     has_right = me < n - 1
     at_end = jnp.logical_not(has_left & has_right)
     beside_end = (me == 1) | (me == n - 2)
     inner = jnp.where(me == 0, 1, n - 2)
     outer = jnp.where(me == 1, 0, n - 1)
+    last = kvh - 1
+    near = jnp.where(me >= n // 2, 0, 1)
 
     barrier = pltpu.get_barrier_semaphore()
 
@@ -68,6 +73,8 @@
     greet({"tp": partner})
     for dx in range(1, n_x):
         greet({"tp": lax.rem(x + dx, n_x) * 2 + core})
+    if direct:
+        greet({"tp": lax.rem(x + 1, n_x) * 2 + 1 - core})
     if detours:
         across = lax.rem(x + 1, n_x) * 2 + core
 
@@ -152,24 +159,49 @@
         )
         return (v * cosine[...] + other * sine[...]).astype(BF16)
 
-    def block_copy(source, g, part, direction):
+    def block_copy(source, g, part, way):
         return pltpu.make_async_remote_copy(
             src_ref=kvbuf.at[source, g, part],
             dst_ref=kvbuf.at[source, g, part],
-            send_sem=gsend.at[direction, source, g, part],
+            send_sem=gsend.at[way, source, g, part],
             recv_sem=grecv.at[source, g, part],
-            device_id={"sp": me + 1 if direction == 0 else me - 1},
+            device_id={"sp": me + 1 - 2 * way},
             device_id_type=MESH,
         )
 
     def spread(g, part):
-        @pl.when(has_right)
+        kept = lend and g == last
+
+        @pl.when((me < n - 2) if kept else has_right)
         def _():
             block_copy(me, g, part, 0).start()
 
-        @pl.when(has_left)
+        @pl.when((me > 1) if kept else has_left)
         def _():
             block_copy(me, g, part, 1).start()
+
+    def lend_queries():
+        return pltpu.make_async_remote_copy(
+            src_ref=qg.at[last],
+            dst_ref=qg.at[kvh],
+            send_sem=lsend.at[0],
+            recv_sem=lrecv.at[0],
+            device_id={"sp": inner},
+            device_id_type=MESH,
+        )
+
+    def return_lent():
+        return [
+            pltpu.make_async_remote_copy(
+                src_ref=ref,
+                dst_ref=ref,
+                send_sem=lsend.at[1 + i],
+                recv_sem=lrecv.at[1 + i],
+                device_id={"sp": outer},
+                device_id_type=MESH,
+            )
+            for i, ref in enumerate((lent, lent_sums))
+        ]
 
     def halo_copy(direction):
         source = rows if direction == 0 else WINDOW
@@ -183,32 +215,58 @@
             device_id_type=MESH,
         )
 
+    def start_halos():
+        @pl.when(has_right)
+        def _():
+            halo_copy(0).start()
+
+        @pl.when(has_left)
+        def _():
+            halo_copy(1).start()
+
+    def turn_queries(g):
+        for u in range(group):
+            q_loads[g * group + u].wait()
+        for u in range(group):
+            part = slice(u * rows, (u + 1) * rows)
+            qg[g, part] = turn(qraw[g, part], qgain_ref[...])
+
+    make_tables()
     for copy in v_loads:
         copy.wait()
-    greeted = has_left.astype(jnp.int32) + has_right.astype(jnp.int32) + n_x
+    greeted = has_left.astype(jnp.int32) + has_right.astype(jnp.int32) + n_x + (1 if direct else 0)
     if detours:
         greeted = greeted + at_end.astype(jnp.int32) + beside_end.astype(jnp.int32)
     pl.semaphore_wait(barrier, greeted)
-    for g in range(kvh):
+    spread(0, 1)
+    if lend:
+        qgain_load.wait()
+        turn_queries(last)
+
+        @pl.when(at_end)
+        def _():
+            lend_queries().start()
+
+    for g in range(1, kvh):
         spread(g, 1)
-
-    make_tables()
+    for copy in w_loads:
+        copy.wait()
+    if lend:
+        @pl.when(at_end)
+        def _():
+            start_halos()
+
     kgain_load.wait()
     for g in range(kvh):
         k_loads[g].wait()
         kvbuf[me, g, 0] = turn(kraw[g], kgain_ref[...])
         spread(g, 0)
-
-    for copy in w_loads:
-        copy.wait()
-
-    @pl.when(has_right)
-    def _():
-        halo_copy(0).start()
-
-    @pl.when(has_left)
-    def _():
-        halo_copy(1).start()
+    if lend:
+        @pl.when(jnp.logical_not(at_end))
+        def _():
+            start_halos()
+    else:
+        start_halos()
 
     @pl.when(jnp.logical_not(has_left))
     def _():
@@ -218,63 +276,166 @@
     def _():
         wkv[:, :, WINDOW + rows :] = jnp.zeros((kvh, 2, WINDOW, HEAD), BF16)
 
-    qgain_load.wait()
-    for copy in q_loads:
-        copy.wait()
-    for g in range(kvh):
-        for u in range(group):
-            part = slice(u * rows, (u + 1) * rows)
-            qg[g, part] = turn(qraw[g, part], qgain_ref[...])
+    if not lend:
+        qgain_load.wait()
+    for g in range(kvh - 1 if lend else kvh):
+        turn_queries(g)
 
     scale = HEAD ** (-0.5)
 
-    def absorb(source, g, first=False):
-        scores = dot_nt(kvbuf[source, g, 0], qg[g]) * scale
+    def absorb(source, g, first=False, slot=None):
+        slot = g if slot is None else slot
+        scores = dot_nt(kvbuf[source, g, 0], qg[slot]) * scale
         block_top = jnp.max(scores, axis=0, keepdims=True)
         if first:
             raised = jnp.exp(scores - block_top)
-            top[g] = block_top
-            total[g] = jnp.sum(raised, axis=0, keepdims=True)
-            acc[g] = dot_tn(kvbuf[source, g, 1], raised.astype(BF16))
+            top[slot] = block_top
+            total[slot] = jnp.sum(raised, axis=0, keepdims=True)
+            acc[slot] = dot_tn(kvbuf[source, g, 1], raised.astype(BF16))
         else:
-            before = top[g]
+            before = top[slot]
             new_top = jnp.maximum(before, block_top)
             fading = jnp.exp(before - new_top)
             raised = jnp.exp(scores - new_top)
-            top[g] = new_top
-            total[g] = total[g] * fading + jnp.sum(raised, axis=0, keepdims=True)
-            acc[g] = acc[g] * fading + dot_tn(kvbuf[source, g, 1], raised.astype(BF16))
+            top[slot] = new_top
+            total[slot] = total[slot] * fading + jnp.sum(raised, axis=0, keepdims=True)
+            acc[slot] = acc[slot] * fading + dot_tn(kvbuf[source, g, 1], raised.astype(BF16))
 
     for g in range(kvh):
         absorb(me, g, True)
 
+    def there(d, way, g):
+        source = me - (1 - 2 * way) * d
+        comes = (source >= 0) & (source < n)
+        if lend and g == last and isinstance(d, int) and d <= 2:
+            comes = comes & jnp.logical_not(at_end)
+        return source, comes
+
+    def piece(d, way, g, part):
+        source, comes = there(d, way, g)
+        target = me + 1 - 2 * way
+
+        @pl.when(comes)
+        def _():
+            block_copy(source, g, part, way).wait_recv()
+            kept = lend and g == last and isinstance(d, int) and d <= 1
+            goes = (target > 0) & (target < n - 1) if kept else (target >= 0) & (target < n)
+
+            @pl.when(goes)
+            def _():
+                block_copy(source, g, part, way).start()
+
+    def take(d, way, g):
+        source, comes = there(d, way, g)
+
+        @pl.when(comes)
+        def _():
+            absorb(source, g)
+
+    def take_all(d, way):
+        if lend and d <= 2:
+            source = me - (1 - 2 * way) * d
+            inside = (source >= 0) & (source < n)
+
+            @pl.when(inside & jnp.logical_not(at_end))
+            def _():
+                for g in range(kvh):
+                    absorb(source, g)
+
+            @pl.when(inside & at_end)
+            def _():
+                for g in range(last):
+                    absorb(source, g)
+        else:
+            source, comes = there(d, way, 0)
+
+            @pl.when(comes)
+            def _():
+                for g in range(kvh):
+                    absorb(source, g)
+
+    def relay_near():
+        far_way = 1 - near
+        for g in range(kvh):
+            piece(1, near, g, 1)
+        piece(1, far_way, 0, 1)
+        for g in range(kvh):
+            if lend and g == last:
+                @pl.when(beside_end)
+                def _():
+                    lend_queries().wait_recv()
+                    absorb(me, last, True, kvh)
+
+            piece(1, near, g, 0)
+        if lend:
+            @pl.when(beside_end)
+            def _():
+                absorb(there(1, near, last)[0], last, False, kvh)
+                lent[...] = (acc[kvh] * (1.0 / total[kvh])).astype(BF16)
+                lent_sums[0] = top[kvh]
+                lent_sums[1] = total[kvh]
+                for copy in return_lent():
+                    copy.start()
+
+        for g in range(1, kvh):
+            piece(1, far_way, g, 1)
+        take_all(1, near)
+
     def relay(d):
+        ways = [near, 1 - near] if not isinstance(d, int) or d < n - n // 2 else [near]
         for part in (1, 0):
             for g in range(kvh):
-                @pl.when(me - d >= 0)
+                for way in ways:
+                    piece(d, way, g, part)
+                if part == 0:
+                    for way in ways:
+                        take(d, way, g)
+                    if n == 4:
+                        @pl.when(at_end)
+                        def _():
+                            finish(g)
+
+    def relay_far_and_second():
+        other = 1 - near
+        ways = (near, other)[: 2 if n > 4 else 1]
+
+        def second(g, part):
+            for way in ways if n > 2 else ():
+                piece(2, way, g, part)
+
+        def take_second(g):
+            for way in ways if n > 2 else ():
+                take(2, way, g)
+
+        window_head(0)
+        piece(1, other, 0, 0)
+        second(0, 1)
+        for g in range(1, kvh):
+            window_head(g)
+        take(1, other, 0)
+        for g in range(1, kvh):
+            piece(1, other, g, 0)
+            second(g, 1)
+            take(1, other, g)
+        window_project(0, chunks)
+        for g in range(kvh):
+            second(g, 0)
+            take_second(g)
+            if n == 4:
+                @pl.when(jnp.logical_not(at_end))
                 def _():
-                    block_copy(me - d, g, part, 0).wait_recv()
-
-                    @pl.when(has_right)
-                    def _():
-                        block_copy(me - d, g, part, 0).start()
-
-                @pl.when(me + d < n)
-                def _():
-                    block_copy(me + d, g, part, 1).wait_recv()
-
-                    @pl.when(has_left)
-                    def _():
-                        block_copy(me + d, g, part, 1).start()
-
-                if part == 0:
-                    @pl.when(me - d >= 0)
-                    def _():
-                        absorb(me - d, g)
-
-                    @pl.when(me + d < n)
-                    def _():
-                        absorb(me + d, g)
+                    finish(g)
+
+    def merge_lent():
+        for copy in return_lent():
+            copy.wait_recv()
+        before = top[last]
+        new_top = jnp.maximum(before, lent_sums[0])
+        fading = jnp.exp(before - new_top)
+        share = jnp.exp(lent_sums[0] - new_top) * lent_sums[1]
+        top[last] = new_top
+        total[last] = total[last] * fading + share
+        acc[last] = acc[last] * fading + lent[...].astype(F32) * share
 
     def put_heads(base, g, value):
         turned = jnp.transpose(value).astype(BF16)
@@ -283,7 +444,10 @@
 
     heads_width = kvh * group * HEAD
 
-    def windowed():
+    def finish(g):
+        put_heads(heads_width, g, acc[g] * (1.0 / total[g]))
+
+    def window_inputs():
         sink_load.wait()
         for copy in wq_loads:
             copy.wait()
@@ -296,53 +460,73 @@
         def _():
             halo_copy(1).wait_recv()
 
-        padded = rows + 2 * WINDOW
+    padded = rows + 2 * WINDOW
+
+    def make_distances():
         key_at = lax.broadcasted_iota(jnp.int32, (padded, span), 0) - WINDOW
-        column = lax.broadcasted_iota(jnp.int32, (padded, span), 1)
+        column = lax.broadcasted_iota(jnp.int32, (1, span), 1)
         distance = jnp.abs(key_at - lax.rem(column, rows))
-        key_place = me * rows + key_at
-        inside = (distance <= WINDOW) & (key_place >= 0) & (key_place < n * rows)
-        far = distance.astype(F32)
+        key_place = me * rows + lax.broadcasted_iota(jnp.int32, (padded, 1), 0) - WINDOW
+        reach = jnp.where((key_place >= 0) & (key_place < n * rows), WINDOW, -1)
+        far[...] = jnp.where(distance <= reach, distance.astype(F32), AWAY)
+
+    def window_head(g):
+        if g == 0:
+            window_inputs()
         member = lax.broadcasted_iota(jnp.int32, (1, span), 1) // rows
+        head = (t * (kvh * group) + g * group + 1 + member).astype(F32)
+        slope = jnp.exp2(head * (-8.0 / QH_A))
+        sink = jnp.zeros((1, span), F32)
+        for u in range(group):
+            sink = jnp.where(member == u, sink_ref[g * group + u], sink)
+        scores = dot_nt(wkv[g, 0], qw[g]) * scale
+        scores = scores - slope * far[...]
+        highest = jnp.maximum(jnp.max(scores, axis=0, keepdims=True), sink)
+        raised = jnp.exp(scores - highest)
+        bottom = jnp.sum(raised, axis=0, keepdims=True) + jnp.exp(sink - highest)
+        weights = (raised * (1.0 / bottom)).astype(BF16)
+        put_heads(0, g, dot_tn(wkv[g, 1], weights))
+
+    def window_project(begin, end):
+        if begin == 0:
+            ww_load.wait()
+        for j in range(begin, end):
+            cols = spans[j]
+            proj[:, cols] = jnp.dot(attn[:, :heads_width], ww[:, cols], preferred_element_type=F32)
+
+    make_distances()
+    if n > 1:
+        relay_near()
+    if n > 1:
+        relay_far_and_second()
+    else:
         for g in range(kvh):
-            head = (t * (kvh * group) + g * group + 1 + member).astype(F32)
-            slope = jnp.exp2(head * (-8.0 / QH_A))
-            sink = jnp.zeros((1, span), F32)
-            for u in range(group):
-                sink = jnp.where(member == u, sink_ref[g * group + u], sink)
-            scores = dot_nt(wkv[g, 0], qw[g]) * scale
-            scores = jnp.where(inside, scores - slope * far, NEGATIVE)
-            highest = jnp.maximum(jnp.max(scores, axis=0, keepdims=True), sink)
-            raised = jnp.exp(scores - highest)
-            bottom = jnp.sum(raised, axis=0, keepdims=True) + jnp.exp(sink - highest)
-            weights = (raised * (1.0 / bottom)).astype(BF16)
-            put_heads(0, g, dot_tn(wkv[g, 1], weights))
-        ww_load.wait()
-        for j in range(chunks):
-            cols = slice(j * width, (j + 1) * width)
-            proj[:, cols] = jnp.dot(attn[:, :heads_width], ww[:, cols], preferred_element_type=F32)
-
-    if n > 1:
-        relay(1)
-    windowed()
+            window_head(g)
+        window_project(0, chunks)
+    if lend:
+        @pl.when(at_end)
+        def _():
+            merge_lent()
+
     if n <= 4:
-        for d in range(2, n):
+        for d in range(3, n):
             relay(d)
     else:
         def relay_step(d, carry):
             relay(d)
             return carry
 
-        lax.fori_loop(2, n, relay_step, 0)
-
-    for g in range(kvh):
-        put_heads(heads_width, g, acc[g] * (1.0 / total[g]))
+        lax.fori_loop(3, n, relay_step, 0)
+
+    if n != 4:
+        for g in range(kvh):
+            finish(g)
     gw_load.wait()
 
     def pair_copy(j):
         return pltpu.make_async_remote_copy(
-            src_ref=pbuf.at[j, 1 - core],
-            dst_ref=dbuf.at[j],
+            src_ref=pbuf.at[j, 1 - core, :, :, sizes[j]],
+            dst_ref=dbuf.at[j, :, :, sizes[j]],
             send_sem=dsend.at[j],
             recv_sem=drecv.at[j],
             device_id={"tp": partner},
@@ -351,11 +535,32 @@
 
     def cross_copy(j, dx):
         return pltpu.make_async_remote_copy(
-            src_ref=sbuf.at[j, dx - 1],
-            dst_ref=rbuf.at[j, dx - 1],
+            src_ref=sbuf.at[j, dx - 1, :, sizes[j]],
+            dst_ref=rbuf.at[j, dx - 1, :, sizes[j]],
             send_sem=xsend.at[j, dx - 1],
             recv_sem=xrecv.at[j, dx - 1],
             device_id={"tp": lax.rem(x + dx, n_x) * 2 + core},
+            device_id_type=MESH,
+        )
+
+    def direct_pair_copy(j):
+        return pltpu.make_async_remote_copy(
+            src_ref=pbuf.at[j, 1 - core, x, :, sizes[j]],
+            dst_ref=dbuf.at[j, x, :, sizes[j]],
+            send_sem=dsend.at[j],
+            recv_sem=drecv.at[j],
+            device_id={"tp": partner},
+            device_id_type=MESH,
+        )
+
+    def direct_copy(j, flip):
+        to = core if flip == 0 else 1 - core
+        return pltpu.make_async_remote_copy(
+            src_ref=pbuf.at[j, to, lax.rem(x + 1, n_x), :, sizes[j]],
+            dst_ref=xbuf.at[j, flip, :, sizes[j]],
+            send_sem=usend.at[j, flip],
+            recv_sem=urecv.at[j, flip],
+            device_id={"tp": lax.rem(x + 1, n_x) * 2 + to},
             device_id_type=MESH,
         )
 
@@ -383,7 +588,8 @@
         pair_copy(j).wait_recv()
         for dx in range(1, n_x):
             other = lax.rem(x + dx, n_x)
-            sbuf[j, dx - 1] = (pbuf[j, core, other].astype(F32) + dbuf[j, other].astype(F32)).astype(BF16)
+            both = pbuf[j, core, other, :, sizes[j]].astype(F32) + dbuf[j, other, :, sizes[j]].astype(F32)
+            sbuf[j, dx - 1, :, sizes[j]] = both.astype(BF16)
             if j in detours:
                 @pl.when(at_end)
                 def _():
@@ -394,32 +600,52 @@
                     cross_copy(j, dx).start()
             else:
                 cross_copy(j, dx).start()
-        own[j] = pbuf[j, core, x].astype(F32) + dbuf[j, x].astype(F32)
-
-    for j in range(chunks):
-        cols = slice(j * width, (j + 1) * width)
-        part = proj[:, cols] + jnp.dot(attn[:, heads_width:], gw[:, cols], preferred_element_type=F32)
+        own[j, :, sizes[j]] = pbuf[j, core, x, :, sizes[j]].astype(F32) + dbuf[j, x, :, sizes[j]].astype(F32)
+
+    def project(j):
+        part = proj[:, spans[j]] + jnp.dot(attn[:, heads_width:], gw[:, spans[j]], preferred_element_type=F32)
         for b in range(n_tp):
-            pbuf[j, b % 2, b // 2] = part[b * out_rows : (b + 1) * out_rows].astype(BF16)
-        pair_copy(j).start()
-        if j >= LAG:
-            pass_on(j - LAG)
-    for j in range(chunks - LAG, chunks):
+            pbuf[j, b % 2, b // 2, :, sizes[j]] = part[b * out_rows : (b + 1) * out_rows].astype(BF16)
+        if j < direct:
+            direct_pair_copy(j).start()
+            for c in range(2):
+                direct_copy(j, c).start()
+        else:
+            pair_copy(j).start()
+
+    for j in range(direct + 1):
+        project(j)
+    project(direct + 1)
+    pass_on(direct)
+    for j in range(direct + 2, chunks):
+        project(j)
+        if j > direct + 2:
+            pass_on(j - 2)
+    for j in range(chunks - 2, chunks):
         pass_on(j)
+
     for j in detours:
         @pl.when(beside_end)
         def _():
             detour_copy(j).wait_recv()
             detour_end_copy(j).start()
 
-    for j in range(chunks):
-        value = own[j]
+    for j in range(direct):
+        direct_pair_copy(j).wait()
+        for c in range(2):
+            direct_copy(j, c).wait()
+        value = pbuf[j, core, x, :, sizes[j]].astype(F32) + dbuf[j, x, :, sizes[j]].astype(F32)
+        for c in range(2):
+            value = value + xbuf[j, c, :, sizes[j]].astype(F32)
+        out_ref[:, spans[j]] = value.astype(BF16)
+    for j in range(direct, chunks):
+        value = own[j, :, sizes[j]]
         for dx in range(1, n_x):
             cross_copy(j, dx).wait_recv()
-            value = value + rbuf[j, dx - 1].astype(F32)
-        out_ref[:, j * width : (j + 1) * width] = value.astype(BF16)
-
-    for j in range(chunks):
+            value = value + rbuf[j, dx - 1, :, sizes[j]].astype(F32)
+        out_ref[:, spans[j]] = value.astype(BF16)
+
+    for j in range(direct, chunks):
         pair_copy(j).wait_send()
         for dx in range(1, n_x):
             cross_copy(j, dx).wait_send()
@@ -436,14 +662,29 @@
     def _():
         halo_copy(1).wait_send()
 
+    if lend:
+        @pl.when(at_end)
+        def _():
+            lend_queries().wait_send()
+
+        @pl.when(beside_end)
+        def _():
+            for copy in return_lent():
+                copy.wait_send()
+
     def drain(source, carry):
         for g in range(kvh):
+            right = has_right & (source <= me)
+            left = has_left & (source >= me)
+            if lend and g == last:
+                right = right & jnp.logical_not((me == n - 2) & (source >= n - 3))
+                left = left & jnp.logical_not((me == 1) & (source <= 2))
             for part in range(2):
-                @pl.when(has_right & (source <= me))
+                @pl.when(right)
                 def _():
                     block_copy(source, g, part, 0).wait_send()
 
-                @pl.when(has_left & (source >= me))
+                @pl.when(left)
                 def _():
                     block_copy(source, g, part, 1).wait_send()
 
@@ -462,16 +703,23 @@
         model = ww.shape[1]
         chunks = 8
         width = model // chunks
+        cuts = [(j * width, (j + 1) * width) for j in range(chunks)]
+        direct = 0
         n_x = n_tp // 2
         out_rows = rows // n_tp
         heads_width = kvh * group * HEAD
         span = group * rows
+        if n_tp == 4 and width > DIRECT:
+            direct = 1
+            cuts = [(0, DIRECT), (DIRECT, width)] + cuts[1:]
+        chunks = len(cuts)
         any_spec = pl.BlockSpec(memory_space=pl.ANY)
         vmem = pl.BlockSpec(memory_space=pltpu.VMEM)
         cross = max(n_x - 1, 1)
-        detours = (1, 3) if n >= 4 and n_x == 2 else ()
+        lend = LEND and n >= 4 and kvh >= 2
+        detours = (3,) if n >= 4 and n_x == 2 else ()
         return pl.pallas_call(
-            functools.partial(kernel, n, n_tp, rows, kvh, group, chunks, detours),
+            functools.partial(kernel, n, n_tp, rows, kvh, group, cuts, direct, detours, lend),
             out_shape=pltpu.VMEM((out_rows, model), BF16),
             in_specs=[any_spec] * 11,
             out_specs=vmem,
@@ -483,15 +731,15 @@
                 pltpu.VMEM((kvh, 2, rows + 2 * WINDOW, HEAD), BF16),
                 pltpu.VMEM((kvh, span, HEAD), BF16),
                 pltpu.VMEM((kvh, rows, HEAD), BF16),
-                pltpu.VMEM((kvh, span, HEAD), BF16),
+                pltpu.VMEM((kvh + lend, span, HEAD), BF16),
                 pltpu.VMEM((n, kvh, 2, rows, HEAD), BF16),
                 pltpu.VMEM(ww.shape, BF16),
                 pltpu.VMEM(gw.shape, BF16),
                 pltpu.VMEM((rows, HEAD), F32),
                 pltpu.VMEM((rows, HEAD), F32),
-                pltpu.VMEM((kvh, 1, span), F32),
-                pltpu.VMEM((kvh, 1, span), F32),
-                pltpu.VMEM((kvh, HEAD, span), F32),
+                pltpu.VMEM((kvh + lend, 1, span), F32),
+                pltpu.VMEM((kvh + lend, 1, span), F32),
+                pltpu.VMEM((kvh + lend, HEAD, span), F32),
                 pltpu.VMEM((rows, 2 * heads_width), BF16),
                 pltpu.VMEM((rows, model), F32),
                 pltpu.VMEM((chunks, 2, n_x, out_rows, width), BF16),
@@ -500,6 +748,10 @@
                 pltpu.VMEM((chunks, cross, out_rows, width), BF16),
                 pltpu.VMEM((chunks, out_rows, width), F32),
                 pltpu.VMEM((max(len(detours), 1), out_rows, width), BF16),
+                pltpu.VMEM((HEAD, span), BF16),
+                pltpu.VMEM((2, 1, span), F32),
+                pltpu.VMEM((max(direct, 1), 2, out_rows, width), BF16),
+                pltpu.VMEM((rows + 2 * WINDOW, span), F32),
                 pltpu.SemaphoreType.DMA((4 * kvh + 2 * kvh * group + 5,)),
                 pltpu.SemaphoreType.DMA((2, n, kvh, 2)),
                 pltpu.SemaphoreType.DMA((n, kvh, 2)),
@@ -511,6 +763,10 @@
                 pltpu.SemaphoreType.DMA((chunks, cross)),
                 pltpu.SemaphoreType.DMA((max(len(detours), 1),)),
                 pltpu.SemaphoreType.DMA((max(len(detours), 1),)),
+                pltpu.SemaphoreType.DMA((3,)),
+                pltpu.SemaphoreType.DMA((3,)),
+                pltpu.SemaphoreType.DMA((max(direct, 1), 2)),
+                pltpu.SemaphoreType.DMA((max(direct, 1), 2)),
             ],
             compiler_params=pltpu.CompilerParams(
                 collective_id=0, has_side_effects=True, vmem_limit_bytes=60 * 1024 * 1024

time: 46.3 us -> 45.4 us (0.981)
  Pallas kernels: 45.3 us -> 44.5 us
    pallas_call x1, Pallas kernels: 45.3 us -> 44.5 us  [per_device(): pl.pallas_call(functools.partial(kernel, n, n_tp, rows, kvh, group, cuts,...]
where the time goes in v3:
time: 45.4 us; the launch traced here: 45.3 us
  Pallas kernels  44.5 us (98%)
  local copies, waits for them, and re-layouts  0.84 us (2%)
    pallas_call x1, Pallas kernels, per_device(): pl.pallas_call(functools.partial(kernel, n, n_tp, rows, kvh, group, cuts,...  44.5 us

profile of v3, /device:TPU:0, one launch (start us, length us, event | category | flops | bytes accessed | tf_op | source)
XLA Modules:
  0.0 45.3 jit_solution(1200478113416902193)
XLA Ops:
  0.0 44.5 %hybrid.1 = bf16[80,4096]{1,0:T(8,128)(2,1)S(1)} custom-call(bf16[320,512]{1,0:T(8,128)(2,1)} %wq_hbm.1, bf16[320,256]{1,0:T(8,128)(2,1)} %wk_hbm.1, bf16[320,256]{1,0:T(8,128)(2,1)} %wv_hbm.1, bf16[320,512]{1,0:T(8,128)(2,1)} %gq_hbm.1, bf16[320,256]{1,0:T(8,128)(2,1)} %gk_hbm.1, bf16[320,256]{1,0:T(8,128)(2,1)} %gv_hbm.1, f32[4]{0:T(128)} %sink_hbm.1, ...), custom_call_target="tpu_custom_call" | custom-call | tf_op jit(solution)/shard_map/hybrid/pallas_call | solution.py:721
  44.5 0.8 %copy.13 = bf16[80,4096]{1,0:T(8,128)(2,1)} copy(bf16[80,4096]{1,0:T(8,128)(2,1)S(1)} %hybrid.1) | data formatting | bytes 1310720

commit v4 on v3

--- a/solution.py
+++ b/solution.py
@@ -566,8 +566,8 @@
 
     def detour_copy(j):
         return pltpu.make_async_remote_copy(
-            src_ref=sbuf.at[j, 0],
-            dst_ref=detour.at[detours.index(j)],
+            src_ref=sbuf.at[j, 0, :, sizes[j]],
+            dst_ref=detour.at[detours.index(j), :, sizes[j]],
             send_sem=xsend.at[j, 0],
             recv_sem=rrecv.at[detours.index(j)],
             device_id={"sp": inner, "tp": across},
@@ -576,8 +576,8 @@
 
     def detour_end_copy(j):
         return pltpu.make_async_remote_copy(
-            src_ref=detour.at[detours.index(j)],
-            dst_ref=rbuf.at[j, 0],
+            src_ref=detour.at[detours.index(j), :, sizes[j]],
+            dst_ref=rbuf.at[j, 0, :, sizes[j]],
             send_sem=rsend.at[detours.index(j)],
             recv_sem=xrecv.at[j, 0],
             device_id={"sp": outer},
@@ -709,9 +709,13 @@
         out_rows = rows // n_tp
         heads_width = kvh * group * HEAD
         span = group * rows
-        if n_tp == 4 and width > DIRECT:
+        if n_tp == 4 and model % 4096 == 0:
             direct = 1
-            cuts = [(0, DIRECT), (DIRECT, width)] + cuts[1:]
+            edges = [0]
+            for part in (1, 3, 4, 5, 4, 4, 4, 4, 3):
+                edges.append(edges[-1] + part * model // 32)
+            cuts = list(zip(edges[:-1], edges[1:]))
+            width = max(end - begin for begin, end in cuts)
         chunks = len(cuts)
         any_spec = pl.BlockSpec(memory_space=pl.ANY)
         vmem = pl.BlockSpec(memory_space=pltpu.VMEM)

time: 45.4 us -> 45.1 us (level)
  no operation moved by 1% of the time
where the time goes in v4:
time: 45.1 us; the launch traced here: 44.9 us
  Pallas kernels  44.1 us (98%)
  local copies, waits for them, and re-layouts  0.84 us (2%)
    pallas_call x1, Pallas kernels, per_device(): pl.pallas_call(functools.partial(kernel, n, n_tp, rows, kvh, group, cuts,...  44.1 us

profile of v4, /device:TPU:0, one launch (start us, length us, event | category | flops | bytes accessed | tf_op | source)
XLA Modules:
  0.0 44.9 jit_solution(11074323765329442688)
XLA Ops:
  0.0 44.1 %hybrid.1 = bf16[80,4096]{1,0:T(8,128)(2,1)S(1)} custom-call(bf16[320,512]{1,0:T(8,128)(2,1)} %wq_hbm.1, bf16[320,256]{1,0:T(8,128)(2,1)} %wk_hbm.1, bf16[320,256]{1,0:T(8,128)(2,1)} %wv_hbm.1, bf16[320,512]{1,0:T(8,128)(2,1)} %gq_hbm.1, bf16[320,256]{1,0:T(8,128)(2,1)} %gk_hbm.1, bf16[320,256]{1,0:T(8,128)(2,1)} %gv_hbm.1, f32[4]{0:T(128)} %sink_hbm.1, ...), custom_call_target="tpu_custom_call" | custom-call | tf_op jit(solution)/shard_map/hybrid/pallas_call | solution.py:725
  44.1 0.8 %copy.13 = bf16[80,4096]{1,0:T(8,128)(2,1)} copy(bf16[80,4096]{1,0:T(8,128)(2,1)S(1)} %hybrid.1) | data formatting | bytes 1310720

commit v5 on v4

--- a/solution.py
+++ b/solution.py
@@ -14,6 +14,7 @@
 GRID_W = 64
 THETA = 10000.0
 AWAY = 1e30
+LOG2E = math.log2(math.e)
 EPSILON = 1e-06
 DIRECT = 128
 LEND = True
@@ -281,22 +282,22 @@
     for g in range(kvh - 1 if lend else kvh):
         turn_queries(g)
 
-    scale = HEAD ** (-0.5)
+    scale = HEAD ** (-0.5) * LOG2E
 
     def absorb(source, g, first=False, slot=None):
         slot = g if slot is None else slot
         scores = dot_nt(kvbuf[source, g, 0], qg[slot]) * scale
         block_top = jnp.max(scores, axis=0, keepdims=True)
         if first:
-            raised = jnp.exp(scores - block_top)
+            raised = jnp.exp2(scores - block_top)
             top[slot] = block_top
             total[slot] = jnp.sum(raised, axis=0, keepdims=True)
             acc[slot] = dot_tn(kvbuf[source, g, 1], raised.astype(BF16))
         else:
             before = top[slot]
             new_top = jnp.maximum(before, block_top)
-            fading = jnp.exp(before - new_top)
-            raised = jnp.exp(scores - new_top)
+            fading = jnp.exp2(before - new_top)
+            raised = jnp.exp2(scores - new_top)
             top[slot] = new_top
             total[slot] = total[slot] * fading + jnp.sum(raised, axis=0, keepdims=True)
             acc[slot] = acc[slot] * fading + dot_tn(kvbuf[source, g, 1], raised.astype(BF16))
@@ -431,8 +432,8 @@
             copy.wait_recv()
         before = top[last]
         new_top = jnp.maximum(before, lent_sums[0])
-        fading = jnp.exp(before - new_top)
-        share = jnp.exp(lent_sums[0] - new_top) * lent_sums[1]
+        fading = jnp.exp2(before - new_top)
+        share = jnp.exp2(lent_sums[0] - new_top) * lent_sums[1]
         top[last] = new_top
         total[last] = total[last] * fading + share
         acc[last] = acc[last] * fading + lent[...].astype(F32) * share
@@ -475,15 +476,15 @@
             window_inputs()
         member = lax.broadcasted_iota(jnp.int32, (1, span), 1) // rows
         head = (t * (kvh * group) + g * group + 1 + member).astype(F32)
-        slope = jnp.exp2(head * (-8.0 / QH_A))
+        slope = jnp.exp2(head * (-8.0 / QH_A)) * LOG2E
         sink = jnp.zeros((1, span), F32)
         for u in range(group):
-            sink = jnp.where(member == u, sink_ref[g * group + u], sink)
+            sink = jnp.where(member == u, sink_ref[g * group + u] * LOG2E, sink)
         scores = dot_nt(wkv[g, 0], qw[g]) * scale
         scores = scores - slope * far[...]
         highest = jnp.maximum(jnp.max(scores, axis=0, keepdims=True), sink)
-        raised = jnp.exp(scores - highest)
-        bottom = jnp.sum(raised, axis=0, keepdims=True) + jnp.exp(sink - highest)
+        raised = jnp.exp2(scores - highest)
+        bottom = jnp.sum(raised, axis=0, keepdims=True) + jnp.exp2(sink - highest)
         weights = (raised * (1.0 / bottom)).astype(BF16)
         put_heads(0, g, dot_tn(wkv[g, 1], weights))
 

time: 45.1 us -> 45.1 us (level)
  no operation moved by 1% of the time
where the time goes in v5:
time: 45.1 us; the launch traced here: 45 us
  Pallas kernels  44.1 us (98%)
  local copies, waits for them, and re-layouts  0.84 us (2%)
    pallas_call x1, Pallas kernels, per_device(): pl.pallas_call(functools.partial(kernel, n, n_tp, rows, kvh, group, cuts,...  44.1 us

profile of v5, /device:TPU:0, one launch (start us, length us, event | category | flops | bytes accessed | tf_op | source)
XLA Modules:
  0.0 45.0 jit_solution(12462152559580822997)
XLA Ops:
  0.0 44.1 %hybrid.1 = bf16[80,4096]{1,0:T(8,128)(2,1)S(1)} custom-call(bf16[320,512]{1,0:T(8,128)(2,1)} %wq_hbm.1, bf16[320,256]{1,0:T(8,128)(2,1)} %wk_hbm.1, bf16[320,256]{1,0:T(8,128)(2,1)} %wv_hbm.1, bf16[320,512]{1,0:T(8,128)(2,1)} %gq_hbm.1, bf16[320,256]{1,0:T(8,128)(2,1)} %gk_hbm.1, bf16[320,256]{1,0:T(8,128)(2,1)} %gv_hbm.1, f32[4]{0:T(128)} %sink_hbm.1, ...), custom_call_target="tpu_custom_call" | custom-call | tf_op jit(solution)/shard_map/hybrid/pallas_call | solution.py:726
  44.1 0.8 %copy.13 = bf16[80,4096]{1,0:T(8,128)(2,1)} copy(bf16[80,4096]{1,0:T(8,128)(2,1)S(1)} %hybrid.1) | data formatting | bytes 1310720
